TPU v7x, 128 devices: a whole 4x4x4 slice. The times are simulated.
128 devices in a mesh: fs: 16 (over z, y), tp: 8 (over x, core).
Axes of the slice: x: 4, y: 4, z: 4, core: 2. Of those that a mesh axis runs over, the one named last changes fastest.
Arguments:
- weights_in: float32 [2, 2048, 5632], P(None, 'fs', 'tp'), may hold values from -6 to 6
- weights_mix: float32 [2048, 2048], P('fs', 'tp'), may hold values from -6 to 6
- momentum_in: float32 [2, 2048, 5632], P(None, 'fs', 'tp'), may hold values from -5 to 5
- momentum_mix: float32 [2048, 2048], P('fs', 'tp'), may hold values from -5 to 5
- grads_in: float32 [2, 2048, 5632], P(None, 'fs', 'tp'), may hold values from -5 to 5
- grads_mix: float32 [2048, 2048], P('fs', 'tp'), may hold values from -5 to 5
Outputs:
- momentum_in_next: float32 [2, 2048, 5632], P(None, 'fs', 'tp')
- momentum_mix_next: float32 [2048, 2048], P('fs', 'tp')
- weights_in_next: float32 [2, 2048, 5632], P(None, 'fs', 'tp')
- weights_mix_next: float32 [2048, 2048], P('fs', 'tp')
- update_in: float32 [2, 2048, 5632], P(None, 'fs', 'tp')
- update_mix: float32 [2048, 2048], P('fs', 'tp')
All inputs are finite; a program needn't handle non-finite values.
Results may differ from a plain program's by a relative error of at most 0.0003.
Values sent between devices are 32-bit elements; how exact they have to be, the bound alone decides.
No kernel may reach another device: no remote copies, remote signals or barrier semaphores. Data moves between devices by JAX's collectives and lax.ppermute only.
A program may use at most 128 MiB of HBM per device.

v0:
```python
import math
import jax
import jax.numpy as jnp
from jax import lax
from jax.sharding import PartitionSpec as P

D = 2048
FF = 5632
ITERS = 3
A_COEF = 3.4445
B_COEF = -4.775
C_COEF = 2.0315
MOMENTUM_DECAY = 0.95
STEP_RATE = 0.02
HIGH = lax.Precision.HIGHEST


def gather_turned(arrays, axis, dims):
    turned = [jnp.moveaxis(a, dim, 0) for a, dim in zip(arrays, dims)]
    both = jnp.concatenate([t.reshape(len(t), -1) for t in turned], axis=1)
    result, at, gathered = (lax.all_gather(both, axis, axis=0, tiled=True), 0, [])
    for t, dim in zip(turned, dims):
        share = result[:, at : at + t[0].size].reshape(-1, *t.shape[1:])
        gathered.append(jnp.moveaxis(share, 0, dim))
        at += t[0].size
    return tuple(gathered)


def rows_for(lines, peers):
    spare = -lines.shape[0] % peers
    if not spare:
        return lines
    return jnp.concatenate([lines, jnp.zeros((spare, *lines.shape[1:]), lines.dtype)])


def sum_by_parts(shard, axis):
    lines = shard.reshape(-1, *shard.shape[1:][-1:])
    own = lax.psum_scatter(
        rows_for(lines, lax.axis_size(axis)), axis, scatter_dimension=0, tiled=True
    )
    whole = lax.all_gather(own, axis).reshape(-1, *lines.shape[1:])
    return lax.slice_in_dim(whole, 0, len(lines)).reshape(shard.shape)


def scale_from(summed):
    return (0.5 * lax.rsqrt(jnp.maximum(summed / D, 1.0)))[:, None, None]


def block_trace(shard, row_start, col_start):
    row_ids = row_start + lax.iota(jnp.int32, shard.shape[1])[:, None]
    col_ids = col_start + lax.iota(jnp.int32, shard.shape[2])[None, :]
    return jnp.sum(jnp.where((row_ids == col_ids)[None], shard, 0.0), axis=(1, 2))


def local(weights_in, weights_mix, momentum_in, momentum_mix, grads_in, grads_mix):
    fs_pos = lax.axis_index("fs")
    tp_pos = lax.axis_index("tp")
    moment_in = MOMENTUM_DECAY * momentum_in + grads_in
    moment_mix = MOMENTUM_DECAY * momentum_mix + grads_mix
    local_in = moment_in
    local_mix = moment_mix[None]
    row_count = local_in.shape[1]
    block_width = local_mix.shape[2]
    for iteration in range(ITERS):
        cols_in, cols_mix = gather_turned((local_in, local_mix), "fs", (1, 1))
        partial_value = jnp.concatenate(
            [
                jnp.einsum("krc,ksc->krs", local_in, cols_in, precision=HIGH),
                jnp.einsum("krc,ksc->krs", local_mix, cols_mix, precision=HIGH),
            ]
        )
        gram_rows = sum_by_parts(partial_value, "tp")
        gram_block = lax.dynamic_slice_in_dim(gram_rows, tp_pos * block_width, block_width, 2)
        if iteration == 0:
            traces = block_trace(gram_block, fs_pos * row_count, tp_pos * block_width)
            scaling = scale_from(lax.psum(traces, ("fs", "tp")))
        factor = scaling if iteration == 0 else jnp.ones_like(scaling)
        gram_cols = lax.all_gather(gram_block, "fs", axis=1, tiled=True)
        square = jnp.einsum("krs,ksc->krc", gram_rows, gram_cols, precision=HIGH)
        poly_mat = factor**2 * B_COEF * gram_block + factor**4 * C_COEF * square
        poly_rows = lax.all_gather(poly_mat, "tp", axis=2, tiled=True)
        local_in = factor[:2] * (
            A_COEF * local_in + jnp.einsum("krs,ksc->krc", poly_rows[:2], cols_in, precision=HIGH)
        )
        local_mix = factor[2:] * (
            A_COEF * local_mix + jnp.einsum("krs,ksc->krc", poly_rows[2:], cols_mix, precision=HIGH)
        )
    step_in = local_in * math.sqrt(max(D, FF))
    step_mix = local_mix[0] * math.sqrt(D)
    return (
        moment_in,
        moment_mix,
        weights_in - STEP_RATE * step_in,
        weights_mix - STEP_RATE * step_mix,
        step_in,
        step_mix,
    )


def solution(mesh):
    in_specs = (
        P(None, "fs", "tp"),
        P("fs", "tp"),
        P(None, "fs", "tp"),
        P("fs", "tp"),
        P(None, "fs", "tp"),
        P("fs", "tp"),
    )
    out_specs = (
        P(None, "fs", "tp"),
        P("fs", "tp"),
        P(None, "fs", "tp"),
        P("fs", "tp"),
        P(None, "fs", "tp"),
        P("fs", "tp"),
    )
    return jax.shard_map(local, mesh=mesh, in_specs=in_specs, out_specs=out_specs, check_vma=False)
```

profile of v0, /device:TPU:1, one launch (start us, length us, event | category | flops | bytes accessed | tf_op | source)
XLA Modules:
  0.0 954.7 jit_solution(4597433947635089846)
XLA Ops:
  10.9 105.9 %all-gather.16.cloned.1.call-done = f32[2048,1664]{0,1:T(8,128)} async-done(((f32[128,1664]{0,1:T(8,128)}), f32[2048,1664]{0,1:T(8,128)}) %all-gather.16.cloned.1.call-update) | async-done | bytes 13631504 | tf_op jit(solution)/shard_map/all_gather | solution.py:21
  116.8 10.4 %slice.58 = f32[2048,1408]{0,1:T(8,128)} slice(f32[2048,1664]{0,1:T(8,128)} %all-gather.16.cloned.1.call-done), slice={[0:2048], [0:1408]} | slice | bytes 23068672 | tf_op jit(solution)/shard_map/slice | solution.py:23
  127.2 9.2 fusion.25
  136.4 2.8 convolution_bitcast_fusion.2
  141.2 33.7 %reduce-scatter.4.cloned.1.call-done = f32[48,2048]{1,0:T(8,128)} async-done(((f32[384,2048]{1,0:T(8,128)}), f32[48,2048]{1,0:T(8,128)}) %reduce-scatter.4.cloned.1.call-update) | async-done | bytes 393232 | tf_op jit(solution)/shard_map/reduce_scatter | solution.py:38
  175.1 31.3 %all-gather.34.cloned.1.call-done = f32[384,2048]{1,0:T(8,128)} async-done(((f32[48,2048]{1,0:T(8,128)}), f32[384,2048]{1,0:T(8,128)}) %all-gather.34.cloned.1.call-update) | async-done | bytes 3145744 | tf_op jit(solution)/shard_map/all_gather | solution.py:41
  208.3 67.5 %psum.7 = f32[3]{0:T(128)S(1)} all-reduce(f32[3]{0:T(128)S(1)} %get-tuple-element.8), channel_id=1, replica_groups=mesh['fs'=16,'tp'=8] {'fs','tp'}, use_global_device_ids=true, to_apply=%region_2.3 | all-reduce | flops 3 | bytes 24 | tf_op jit(solution)/shard_map/psum | solution.py:76
  275.8 8.2 fusion.10
  284.9 23.8 %all-gather.20.cloned.1.call-done = f32[3,128,2048]{2,1,0:T(8,128)} async-done(((f32[3,128,256]{2,1,0:T(8,128)}), f32[3,128,2048]{2,1,0:T(8,128)}) %all-gather.20.cloned.1.call-update) | async-done | bytes 3145744 | tf_op jit(solution)/shard_map/all_gather | solution.py:81
  308.7 4.8 fusion.16
  313.6 13.0 %fusion.9 = f32[2,128,704]{1,2,0:T(8,128)S(1)} fusion(f32[3,128,2048]{2,1,0:T(8,128)} %all-gather.20.cloned.1.call-done, f32[2,2048,704]{1,2,0:T(8,128)} %bitcast.65, f32[2,128,704]{1,2,0:T(8,128)S(1)} %multiply_add_fusion, f32[2]{0:T(128)S(1)} %bitcast.82), kind=kOutput, calls=%fused_computation.18 | convolution fusion | flops 4429725696 | bytes 16121864 | tf_op jit(solution)/shard_map/krs,ksc->krc/dot_general | solution.py:83
  327.9 102.1 %all-gather.22.cloned.1.call-done = f32[2048,1664]{0,1:T(8,128)} async-done(((f32[128,1664]{0,1:T(8,128)}), f32[2048,1664]{0,1:T(8,128)}) %all-gather.22.cloned.1.call-update) | async-done | bytes 13631504 | tf_op jit(solution)/shard_map/all_gather | solution.py:21
  429.9 10.4 %slice.61 = f32[2048,1408]{0,1:T(8,128)} slice(f32[2048,1664]{0,1:T(8,128)} %all-gather.22.cloned.1.call-done), slice={[0:2048], [0:1408]} | slice | bytes 23068672 | tf_op jit(solution)/shard_map/slice | solution.py:23
  440.3 9.2 fusion.26
  449.5 2.8 convolution_bitcast_fusion.1
  454.4 33.7 %reduce-scatter.6.cloned.1.call-done = f32[48,2048]{1,0:T(8,128)} async-done(((f32[384,2048]{1,0:T(8,128)}), f32[48,2048]{1,0:T(8,128)}) %reduce-scatter.6.cloned.1.call-update) | async-done | bytes 393232 | tf_op jit(solution)/shard_map/reduce_scatter | solution.py:38
  488.1 31.5 %all-gather.36.cloned.1.call-done = f32[384,2048]{1,0:T(8,128)} async-done(((f32[48,2048]{1,0:T(8,128)}), f32[384,2048]{1,0:T(8,128)}) %all-gather.36.cloned.1.call-update) | async-done | bytes 3145744 | tf_op jit(solution)/shard_map/all_gather | solution.py:41
  521.4 61.7 %all-gather.24.cloned.1.call-done = f32[3,2048,256]{2,1,0:T(8,128)} async-done(((f32[3,128,256]{2,1,0:T(8,128)}), f32[3,2048,256]{2,1,0:T(8,128)}) %all-gather.24.cloned.1.call-update) | async-done | bytes 6291472 | tf_op jit(solution)/shard_map/all_gather | solution.py:78
  583.1 8.2 fusion.11
  591.8 27.5 %all-gather.26.cloned.1.call-done = f32[3,128,2048]{2,1,0:T(8,128)} async-done(((f32[3,128,256]{2,1,0:T(8,128)}), f32[3,128,2048]{2,1,0:T(8,128)}) %all-gather.26.cloned.1.call-update) | async-done | bytes 3145744 | tf_op jit(solution)/shard_map/all_gather | solution.py:81
  619.3 4.1 fusion.19
  623.5 13.0 %convolution_add_fusion.1 = f32[2,128,704]{1,2,0:T(8,128)S(1)} fusion(f32[3,128,2048]{2,1,0:T(8,128)} %all-gather.26.cloned.1.call-done, f32[2,2048,704]{1,2,0:T(8,128)} %bitcast.69, f32[2,128,704]{1,2,0:T(8,128)S(1)} %fusion.9), kind=kOutput, calls=%fused_computation.16 | convolution fusion | flops 4429545472 | bytes 16121856 | tf_op jit(solution)/shard_map/krs,ksc->krc/dot_general | solution.py:83
  637.6 102.3 %all-gather.28.cloned.1.call-done = f32[2048,1664]{0,1:T(8,128)} async-done(((f32[128,1664]{0,1:T(8,128)}), f32[2048,1664]{0,1:T(8,128)}) %all-gather.28.cloned.1.call-update) | async-done | bytes 13631504 | tf_op jit(solution)/shard_map/all_gather | solution.py:21
  739.8 10.4 %slice.64 = f32[2048,1408]{0,1:T(8,128)} slice(f32[2048,1664]{0,1:T(8,128)} %all-gather.28.cloned.1.call-done), slice={[0:2048], [0:1408]} | slice | bytes 23068672 | tf_op jit(solution)/shard_map/slice | solution.py:23
  750.2 9.2 fusion.27
  764.2 33.7 %reduce-scatter.8.cloned.1.call-done = f32[48,2048]{1,0:T(8,128)} async-done(((f32[384,2048]{1,0:T(8,128)}), f32[48,2048]{1,0:T(8,128)}) %reduce-scatter.8.cloned.1.call-update) | async-done | bytes 393232 | tf_op jit(solution)/shard_map/reduce_scatter | solution.py:38
  798.0 31.5 %all-gather.38.cloned.1.call-done = f32[384,2048]{1,0:T(8,128)} async-done(((f32[48,2048]{1,0:T(8,128)}), f32[384,2048]{1,0:T(8,128)}) %all-gather.38.cloned.1.call-update) | async-done | bytes 3145744 | tf_op jit(solution)/shard_map/all_gather | solution.py:41
  831.5 61.4 %all-gather.30.cloned.1.call-done = f32[3,2048,256]{2,1,0:T(8,128)} async-done(((f32[3,128,256]{2,1,0:T(8,128)}), f32[3,2048,256]{2,1,0:T(8,128)}) %all-gather.30.cloned.1.call-update) | async-done | bytes 6291472 | tf_op jit(solution)/shard_map/all_gather | solution.py:78
  892.8 8.2 fusion.12
  901.1 27.9 %all-gather.32.cloned.1.call-done = f32[3,128,2048]{2,1,0:T(8,128)} async-done(((f32[3,128,256]{2,1,0:T(8,128)}), f32[3,128,2048]{2,1,0:T(8,128)}) %all-gather.32.cloned.1.call-update) | async-done | bytes 3145744 | tf_op jit(solution)/shard_map/all_gather | solution.py:81
  929.0 5.0 broadcast_multiply_fusion.1
  934.0 13.9 %broadcast_multiply_fusion = (f32[2,128,704]{1,2,0:T(8,128)}, f32[2,128,704]{1,2,0:T(8,128)}) fusion(f32[2,128,704]{1,2,0:T(8,128)S(1)} %copy-done.3, f32[3,128,2048]{2,1,0:T(8,128)S(1)} %copy-done.1, f32[2,2048,704]{1,2,0:T(8,128)} %bitcast.67, f32[2,128,704]{1,2,0:T(8,128)S(1)} %convolution_add_fusion.1), kind=kOutput, calls=%fused_computation.38 | convolution fusion | flops 4430086144 | bytes 17563648 | tf_op jit(solution)/shard_map/krs,ksc->krc/dot_general | solution.py:83
  (62 shorter events, 22.2 us)
Async XLA Ops:
  7.2 109.6 %all-gather.16.cloned.1.call-start = ((), (), s32[]{:S(2)}) async-start(), calls=%async_computation.3 | async-start | bytes 14483456 | tf_op jit(solution)/shard_map/all_gather | solution.py:21
  8.2 300.5 %copy-start.2 = (f32[128,256]{1,0:T(8,128)}, f32[128,256]{1,0:T(8,128)S(1)}, u32[]{:S(2)}) copy-start(f32[128,256]{1,0:T(8,128)S(1)} %multiply_add_fusion.1) | copy-start | bytes 393220
  9.7 303.9 %copy-start = (f32[2,128,704]{1,2,0:T(8,128)}, f32[2,128,704]{1,2,0:T(8,128)S(1)}, u32[]{:S(2)}) copy-start(f32[2,128,704]{1,2,0:T(8,128)S(1)} %multiply_add_fusion) | copy-start | bytes 2162692
  10.8 164.1 %reduce-scatter.4.cloned.1.call-start = ((), (), s32[]{:S(2)}) async-start(), calls=%async_computation.4 | async-start | bytes 3538944 | tf_op jit(solution)/shard_map/reduce_scatter | solution.py:38
  141.2 65.3 %all-gather.34.cloned.1.call-start = ((), (), s32[]{:S(2)}) async-start(), calls=%async_computation.15 | async-start | bytes 3538944 | tf_op jit(solution)/shard_map/all_gather | solution.py:41
  174.9 100.9 %all-gather.18.cloned.1.call-start = ((), (), s32[]{:S(2)}) async-start(), calls=%async_computation.5 | async-start | bytes 6684672 | tf_op jit(solution)/shard_map/all_gather | solution.py:78
  208.2 100.5 %all-gather.20.cloned.1.call-start = ((), (), s32[]{:S(2)}) async-start(), calls=%async_computation.6 | async-start | bytes 3538944 | tf_op jit(solution)/shard_map/all_gather | solution.py:81
  284.1 145.9 %all-gather.22.cloned.1.call-start = ((), (), s32[]{:S(2)}) async-start(), calls=%async_computation.7 | async-start | bytes 14483456 | tf_op jit(solution)/shard_map/all_gather | solution.py:21
  327.6 160.4 %reduce-scatter.6.cloned.1.call-start = ((), (), s32[]{:S(2)}) async-start(), calls=%async_computation.8 | async-start | bytes 3538944 | tf_op jit(solution)/shard_map/reduce_scatter | solution.py:38
  454.3 65.3 %all-gather.36.cloned.1.call-start = ((), (), s32[]{:S(2)}) async-start(), calls=%async_computation.16 | async-start | bytes 3538944 | tf_op jit(solution)/shard_map/all_gather | solution.py:41
  488.1 95.1 %all-gather.24.cloned.1.call-start = ((), (), s32[]{:S(2)}) async-start(), calls=%async_computation.9 | async-start | bytes 6684672 | tf_op jit(solution)/shard_map/all_gather | solution.py:78
  521.4 97.9 %all-gather.26.cloned.1.call-start = ((), (), s32[]{:S(2)}) async-start(), calls=%async_computation.10 | async-start | bytes 3538944 | tf_op jit(solution)/shard_map/all_gather | solution.py:81
  591.3 148.5 %all-gather.28.cloned.1.call-start = ((), (), s32[]{:S(2)}) async-start(), calls=%async_computation.11 | async-start | bytes 14483456 | tf_op jit(solution)/shard_map/all_gather | solution.py:21
  637.5 160.4 %reduce-scatter.8.cloned.1.call-start = ((), (), s32[]{:S(2)}) async-start(), calls=%async_computation.12 | async-start | bytes 3538944 | tf_op jit(solution)/shard_map/reduce_scatter | solution.py:38
  764.2 65.3 %all-gather.38.cloned.1.call-start = ((), (), s32[]{:S(2)}) async-start(), calls=%async_computation.17 | async-start | bytes 3538944 | tf_op jit(solution)/shard_map/all_gather | solution.py:41
  797.9 94.9 %all-gather.30.cloned.1.call-start = ((), (), s32[]{:S(2)}) async-start(), calls=%async_computation.13 | async-start | bytes 6684672 | tf_op jit(solution)/shard_map/all_gather | solution.py:78
  831.2 97.8 %copy-start.4 = (f32[128,256]{1,0:T(8,128)S(1)}, f32[128,256]{1,0:T(8,128)}, u32[]{:S(2)}) copy-start(f32[128,256]{1,0:T(8,128)} %param.7) | copy-start | bytes 393220
  831.3 97.8 %all-gather.32.cloned.1.call-start = ((), (), s32[]{:S(2)}) async-start(), calls=%async_computation.14 | async-start | bytes 3538944 | tf_op jit(solution)/shard_map/all_gather | solution.py:81
  901.1 33.0 %copy-start.3 = (f32[2,128,704]{1,2,0:T(8,128)S(1)}, f32[2,128,704]{1,2,0:T(8,128)}, u32[]{:S(2)}) copy-start(f32[2,128,704]{1,2,0:T(8,128)} %param.6) | copy-start | bytes 2162692
  929.0 5.0 copy-start.1
Sparse Core Ops, SparseCore 0:
  10.9 105.7 all-gather.15
  141.3 33.5 reduce-scatter.3
  176.6 29.8 all-gather.33
  209.0 61.3 all-gather.17
  284.2 24.4 all-gather.19
  327.7 102.1 all-gather.21
  454.4 33.5 reduce-scatter.5
  489.7 29.8 all-gather.35
  522.3 60.7 all-gather.23
  591.5 27.7 all-gather.25
  637.6 102.1 all-gather.27
  764.3 33.5 reduce-scatter.7
  799.6 29.8 all-gather.37
  832.0 60.7 all-gather.29
  901.2 27.7 all-gather.31
where the time goes:
time: 963 us; the launch traced here: 955 us
  waiting for transfers between devices  708 us (74%)
  matrix products  114 us (12%)
  blocking collectives  67.5 us (7%)
  local copies, waits for them, and re-layouts  35.7 us (4%)
  between operations  14.3 us (1%)
  other arithmetic  13.1 us (1%)
    all_gather x3, waiting for transfers between devices, gather_turned(): lax.all_gather(both, axis, axis=0, tiled=True)  310 us
    all_gather x3, waiting for transfers between devices, local(): gram_cols = lax.all_gather(gram_block, 'fs', axis=1, tiled=True)  123 us
    reduce_scatter x3, waiting for transfers between devices, sum_by_parts(): lax.psum_scatter(rows_for(lines, lax.axis_size(axis)), axis, scatter_dime...  101 us
    all_gather x3, waiting for transfers between devices, sum_by_parts(): whole = lax.all_gather(own, axis).reshape(-1, *lines.shape[1:])  94.3 us
    all_gather x3, waiting for transfers between devices, local(): poly_rows = lax.all_gather(poly_mat, 'tp', axis=2, tiled=True)  79.3 us
    psum x1, blocking collectives, local(): scaling = scale_from(lax.psum(traces, ('fs', 'tp')))  67.5 us
    dot_general x3, matrix products, local(): jnp.einsum('krs,ksc->krc', poly_rows[:2], cols_in, precision=HIGH)  39.9 us
    slice x3, local copies, waits for them, and re-layouts, gather_turned(): share = result[:, at:at + t[0].size].reshape(-1, *t.shape[1:])  31.2 us
  transfers between devices with their start and end apart: 15, of which 14 were waited for; matrix products, arithmetic and copies ran while one was open for 0% of the time, Pallas kernels for 0%

commit v1 on v0

--- a/solution.py
+++ b/solution.py
@@ -75,7 +75,9 @@
             traces = block_trace(gram_block, fs_pos * row_count, tp_pos * block_width)
             scaling = scale_from(lax.psum(traces, ("fs", "tp")))
         factor = scaling if iteration == 0 else jnp.ones_like(scaling)
-        gram_cols = lax.all_gather(gram_block, "fs", axis=1, tiled=True)
+        gram_cols = jnp.concatenate(
+            lax.all_to_all(jnp.stack([gram_block] * lax.axis_size("fs")), "fs", 0, 0), axis=1
+        )
         square = jnp.einsum("krs,ksc->krc", gram_rows, gram_cols, precision=HIGH)
         poly_mat = factor**2 * B_COEF * gram_block + factor**4 * C_COEF * square
         poly_rows = lax.all_gather(poly_mat, "tp", axis=2, tiled=True)

time: 963 us -> 1080 us (1.12)
  blocking collectives: 67.5 us -> 306 us
  waiting for transfers between devices: 708 us -> 571 us
  starting transfers between devices: 1.57 us -> 17.6 us
  matrix products: 114 us -> 103 us
    all_to_all x0 -> x2, blocking collectives: none -> 158 us  [local(): lax.all_to_all(jnp.stack([gram_block] * lax.axis_size('fs')), 'fs', 0, 0)]
    all_gather x3 -> x0, waiting for transfers between devices: 123 us -> none  [local(): gram_cols = lax.all_gather(gram_block, 'fs', axis=1, tiled=True)]
    psum x1, blocking collectives: 67.5 us -> 148 us  [local(): scaling = scale_from(lax.psum(traces, ('fs', 'tp')))]
    all_gather x3, waiting for transfers between devices: 79.3 us -> 65.4 us  [local(): poly_rows = lax.all_gather(poly_mat, 'tp', axis=2, tiled=True)]
    dot_general x3, matrix products: 24.6 us -> 13.7 us  [local(): square = jnp.einsum('krs,ksc->krc', gram_rows, gram_cols, precision=HIGH)]
  transfers between devices with their start and end apart: 15 -> 13, of which waited for: 14 -> 12; matrix products, arithmetic and copies ran while one was open for 0% -> 0% of each run, Pallas kernels for 0% -> 0%
where the time goes in v1:
time: 1080 us; the launch traced here: 1070 us
  waiting for transfers between devices  571 us (53%)
  blocking collectives  306 us (28%)
  matrix products  103 us (10%)
  local copies, waits for them, and re-layouts  46.5 us (4%)
  starting transfers between devices  17.6 us (2%)
  between operations  14.7 us (1%)
  other arithmetic  12.5 us (1%)
    all_gather x3, waiting for transfers between devices, gather_turned(): lax.all_gather(both, axis, axis=0, tiled=True)  310 us
    all_to_all x2, blocking collectives, local(): lax.all_to_all(jnp.stack([gram_block] * lax.axis_size('fs')), 'fs', 0, 0)  158 us
    psum x1, blocking collectives, local(): scaling = scale_from(lax.psum(traces, ('fs', 'tp')))  148 us
    reduce_scatter x3, waiting for transfers between devices, sum_by_parts(): lax.psum_scatter(rows_for(lines, lax.axis_size(axis)), axis, scatter_dime...  101 us
    all_gather x3, waiting for transfers between devices, sum_by_parts(): whole = lax.all_gather(own, axis).reshape(-1, *lines.shape[1:])  94.4 us
    all_gather x3, waiting for transfers between devices, local(): poly_rows = lax.all_gather(poly_mat, 'tp', axis=2, tiled=True)  65.4 us
    dot_general x3, matrix products, local(): jnp.einsum('krs,ksc->krc', poly_rows[:2], cols_in, precision=HIGH)  39.9 us
    slice x3, local copies, waits for them, and re-layouts, gather_turned(): share = result[:, at:at + t[0].size].reshape(-1, *t.shape[1:])  31.2 us
  transfers between devices with their start and end apart: 13, of which 12 were waited for; matrix products, arithmetic and copies ran while one was open for 0% of the time, Pallas kernels for 0%

profile of v1, /device:TPU:1, one launch (start us, length us, event | category | flops | bytes accessed | tf_op | source)
XLA Modules:
  0.0 1072.1 jit_solution(5101522628919980542)
XLA Ops:
  10.9 105.9 %all-gather.13.cloned.1.call-done = f32[2048,1664]{0,1:T(8,128)} async-done(((f32[128,1664]{0,1:T(8,128)}), f32[2048,1664]{0,1:T(8,128)}) %all-gather.13.cloned.1.call-update) | async-done | bytes 13631504 | tf_op jit(solution)/shard_map/all_gather | solution.py:21
  116.8 10.4 slice.58
  127.2 9.2 fusion.25
  141.2 33.7 %reduce-scatter.4.cloned.1.call-done = f32[48,2048]{1,0:T(8,128)} async-done(((f32[384,2048]{1,0:T(8,128)}), f32[48,2048]{1,0:T(8,128)}) %reduce-scatter.4.cloned.1.call-update) | async-done | bytes 393232 | tf_op jit(solution)/shard_map/reduce_scatter | solution.py:38
  175.0 31.4 %all-gather.25.cloned.1.call-done = f32[384,2048]{1,0:T(8,128)} async-done(((f32[48,2048]{1,0:T(8,128)}), f32[384,2048]{1,0:T(8,128)}) %all-gather.25.cloned.1.call-update) | async-done | bytes 3145744 | tf_op jit(solution)/shard_map/all_gather | solution.py:41
  211.0 6.7 all-to-all-start
  217.8 147.8 %psum.7 = f32[3]{0:T(128)S(1)} all-reduce(f32[3]{0:T(128)S(1)} %get-tuple-element.8), channel_id=1, replica_groups=mesh['fs'=16,'tp'=8] {'fs','tp'}, use_global_device_ids=true, to_apply=%region_2.3 | all-reduce | flops 3 | bytes 24 | tf_op jit(solution)/shard_map/psum | solution.py:76
  369.3 4.6 fusion.10
  374.7 24.9 %all-gather.15.cloned.1.call-done = f32[3,128,2048]{2,1,0:T(8,128)} async-done(((f32[3,128,256]{2,1,0:T(8,128)}), f32[3,128,2048]{2,1,0:T(8,128)}) %all-gather.15.cloned.1.call-update) | async-done | bytes 3145744 | tf_op jit(solution)/shard_map/all_gather | solution.py:83
  399.6 4.8 fusion.16
  404.5 13.0 %fusion.9 = f32[2,128,704]{1,2,0:T(8,128)S(1)} fusion(f32[3,128,2048]{2,1,0:T(8,128)} %all-gather.15.cloned.1.call-done, f32[2,2048,704]{1,2,0:T(8,128)} %bitcast.71, f32[2,128,704]{1,2,0:T(8,128)S(1)} %multiply_add_fusion, f32[2]{0:T(128)S(1)} %bitcast.93), kind=kOutput, calls=%fused_computation.18 | convolution fusion | flops 4429725696 | bytes 16121864 | tf_op jit(solution)/shard_map/krs,ksc->krc/dot_general | solution.py:85
  418.9 101.9 %all-gather.17.cloned.1.call-done = f32[2048,1664]{0,1:T(8,128)} async-done(((f32[128,1664]{0,1:T(8,128)}), f32[2048,1664]{0,1:T(8,128)}) %all-gather.17.cloned.1.call-update) | async-done | bytes 13631504 | tf_op jit(solution)/shard_map/all_gather | solution.py:21
  520.9 10.4 slice.61
  531.3 9.2 fusion.26
  545.3 33.6 %reduce-scatter.6.cloned.1.call-done = f32[48,2048]{1,0:T(8,128)} async-done(((f32[384,2048]{1,0:T(8,128)}), f32[48,2048]{1,0:T(8,128)}) %reduce-scatter.6.cloned.1.call-update) | async-done | bytes 393232 | tf_op jit(solution)/shard_map/reduce_scatter | solution.py:38
  579.0 31.5 %all-gather.27.cloned.1.call-done = f32[384,2048]{1,0:T(8,128)} async-done(((f32[48,2048]{1,0:T(8,128)}), f32[384,2048]{1,0:T(8,128)}) %all-gather.27.cloned.1.call-update) | async-done | bytes 3145744 | tf_op jit(solution)/shard_map/all_gather | solution.py:41
  612.3 79.1 %all_to_all.15 = f32[16,3,128,256]{3,2,1,0:T(8,128)S(1)} all-to-all(f32[16,3,128,256]{3,2,1,0:T(8,128)S(1)} %stack.7), channel_id=1, replica_groups=mesh['fs'=16,'tp'=8] {'fs'}, dimensions={0} | all-to-all | bytes 12582912 | tf_op jit(solution)/shard_map/all_to_all | solution.py:79
  693.3 4.6 fusion.11
  697.9 9.9 all-gather.21.cloned.1.call-start
  707.8 15.3 %all-gather.19.cloned.1.call-done = f32[3,128,2048]{2,1,0:T(8,128)} async-done(((f32[3,128,256]{2,1,0:T(8,128)}), f32[3,128,2048]{2,1,0:T(8,128)}) %all-gather.19.cloned.1.call-update) | async-done | bytes 3145744 | tf_op jit(solution)/shard_map/all_gather | solution.py:83
  723.1 4.1 fusion.19
  727.3 13.0 %convolution_add_fusion.1 = f32[2,128,704]{1,2,0:T(8,128)S(1)} fusion(f32[3,128,2048]{2,1,0:T(8,128)} %all-gather.19.cloned.1.call-done, f32[2,2048,704]{1,2,0:T(8,128)} %bitcast.75, f32[2,128,704]{1,2,0:T(8,128)S(1)} %fusion.9), kind=kOutput, calls=%fused_computation.16 | convolution fusion | flops 4429545472 | bytes 16121856 | tf_op jit(solution)/shard_map/krs,ksc->krc/dot_general | solution.py:85
  741.4 102.3 %all-gather.21.cloned.1.call-done = f32[2048,1664]{0,1:T(8,128)} async-done(((f32[128,1664]{0,1:T(8,128)}), f32[2048,1664]{0,1:T(8,128)}) %all-gather.21.cloned.1.call-update) | async-done | bytes 13631504 | tf_op jit(solution)/shard_map/all_gather | solution.py:21
  843.7 10.4 slice.64
  854.1 9.2 fusion.27
  868.1 33.7 %reduce-scatter.8.cloned.1.call-done = f32[48,2048]{1,0:T(8,128)} async-done(((f32[384,2048]{1,0:T(8,128)}), f32[48,2048]{1,0:T(8,128)}) %reduce-scatter.8.cloned.1.call-update) | async-done | bytes 393232 | tf_op jit(solution)/shard_map/reduce_scatter | solution.py:38
  901.8 31.5 %all-gather.29.cloned.1.call-done = f32[384,2048]{1,0:T(8,128)} async-done(((f32[48,2048]{1,0:T(8,128)}), f32[384,2048]{1,0:T(8,128)}) %all-gather.29.cloned.1.call-update) | async-done | bytes 3145744 | tf_op jit(solution)/shard_map/all_gather | solution.py:41
  935.1 79.3 %all_to_all.16 = f32[16,3,128,256]{3,2,1,0:T(8,128)S(1)} all-to-all(f32[16,3,128,256]{3,2,1,0:T(8,128)S(1)} %stack.8), channel_id=1, replica_groups=mesh['fs'=16,'tp'=8] {'fs'}, dimensions={0} | all-to-all | bytes 12582912 | tf_op jit(solution)/shard_map/all_to_all | solution.py:79
  1016.3 4.6 fusion.12
  1020.9 25.2 %all-gather.23.cloned.1.call-done = f32[3,128,2048]{2,1,0:T(8,128)} async-done(((f32[3,128,256]{2,1,0:T(8,128)}), f32[3,128,2048]{2,1,0:T(8,128)}) %all-gather.23.cloned.1.call-update) | async-done | bytes 3145744 | tf_op jit(solution)/shard_map/all_gather | solution.py:83
  1046.1 5.0 broadcast_multiply_fusion.1
  1051.1 13.9 %broadcast_multiply_fusion = (f32[2,128,704]{1,2,0:T(8,128)}, f32[2,128,704]{1,2,0:T(8,128)}) fusion(f32[2,128,704]{1,2,0:T(8,128)S(1)} %copy-done.6, f32[3,128,2048]{2,1,0:T(8,128)S(1)} %copy-done.1, f32[2,2048,704]{1,2,0:T(8,128)} %bitcast.73, f32[2,128,704]{1,2,0:T(8,128)S(1)} %convolution_add_fusion.1), kind=kOutput, calls=%fused_computation.38 | convolution fusion | flops 4430086144 | bytes 17563648 | tf_op jit(solution)/shard_map/krs,ksc->krc/dot_general | solution.py:85
  (69 shorter events, 37.5 us)
Async XLA Ops:
  7.2 109.6 %all-gather.13.cloned.1.call-start = ((), (), s32[]{:S(2)}) async-start(), calls=%async_computation.6 | async-start | bytes 14483456 | tf_op jit(solution)/shard_map/all_gather | solution.py:21
  8.2 391.4 %copy-start.5 = (f32[128,256]{1,0:T(8,128)}, f32[128,256]{1,0:T(8,128)S(1)}, u32[]{:S(2)}) copy-start(f32[128,256]{1,0:T(8,128)S(1)} %multiply_add_fusion.1) | copy-start | bytes 393220
  9.7 394.8 %copy-start = (f32[2,128,704]{1,2,0:T(8,128)}, f32[2,128,704]{1,2,0:T(8,128)S(1)}, u32[]{:S(2)}) copy-start(f32[2,128,704]{1,2,0:T(8,128)S(1)} %multiply_add_fusion) | copy-start | bytes 2162692
  10.8 164.0 %reduce-scatter.4.cloned.1.call-start = ((), (), s32[]{:S(2)}) async-start(), calls=%async_computation.7 | async-start | bytes 3538944 | tf_op jit(solution)/shard_map/reduce_scatter | solution.py:38
  141.1 65.3 %all-gather.25.cloned.1.call-start = ((), (), s32[]{:S(2)}) async-start(), calls=%async_computation.15 | async-start | bytes 3538944 | tf_op jit(solution)/shard_map/all_gather | solution.py:41
  211.0 154.6 %all-to-all-start = ((f32[16,3,128,256]{3,2,1,0:T(8,128)}), f32[16,3,128,256]{3,2,1,0:T(8,128)}, u32[]{:S(2)}, u32[]{:S(2)}) async-start(f32[16,3,128,256]{3,2,1,0:T(8,128)} %stack.6), calls=%async_computation.1 | async-start | bytes 12582912 | tf_op jit(solution)/shard_map/all_to_all | solution.py:79
  217.8 181.9 %all-gather.15.cloned.1.call-start = ((), (), s32[]{:S(2)}) async-start(), calls=%async_computation.8 | async-start | bytes 3538944 | tf_op jit(solution)/shard_map/all_gather | solution.py:83
  365.6 3.7 copy-start.2
  373.9 147.0 %all-gather.17.cloned.1.call-start = ((), (), s32[]{:S(2)}) async-start(), calls=%async_computation.9 | async-start | bytes 14483456 | tf_op jit(solution)/shard_map/all_gather | solution.py:21
  418.6 160.4 %reduce-scatter.6.cloned.1.call-start = ((), (), s32[]{:S(2)}) async-start(), calls=%async_computation.10 | async-start | bytes 3538944 | tf_op jit(solution)/shard_map/reduce_scatter | solution.py:38
  545.2 65.2 %all-gather.27.cloned.1.call-start = ((), (), s32[]{:S(2)}) async-start(), calls=%async_computation.16 | async-start | bytes 3538944 | tf_op jit(solution)/shard_map/all_gather | solution.py:41
  579.0 144.1 %all-gather.19.cloned.1.call-start = ((), (), s32[]{:S(2)}) async-start(), calls=%async_computation.11 | async-start | bytes 3538944 | tf_op jit(solution)/shard_map/all_gather | solution.py:83
  691.4 1.9 copy-start.4
  697.9 145.8 %all-gather.21.cloned.1.call-start = ((), (), s32[]{:S(2)}) async-start(), calls=%async_computation.12 | async-start | bytes 14483456 | tf_op jit(solution)/shard_map/all_gather | solution.py:21
  741.3 160.4 %reduce-scatter.8.cloned.1.call-start = ((), (), s32[]{:S(2)}) async-start(), calls=%async_computation.13 | async-start | bytes 3538944 | tf_op jit(solution)/shard_map/reduce_scatter | solution.py:38
  868.0 65.3 %all-gather.29.cloned.1.call-start = ((), (), s32[]{:S(2)}) async-start(), calls=%async_computation.17 | async-start | bytes 3538944 | tf_op jit(solution)/shard_map/all_gather | solution.py:41
  901.8 144.3 %all-gather.23.cloned.1.call-start = ((), (), s32[]{:S(2)}) async-start(), calls=%async_computation.14 | async-start | bytes 3538944 | tf_op jit(solution)/shard_map/all_gather | solution.py:83
  1014.4 1.9 copy-start.3
  1016.3 29.8 %copy-start.7 = (f32[128,256]{1,0:T(8,128)S(1)}, f32[128,256]{1,0:T(8,128)}, u32[]{:S(2)}) copy-start(f32[128,256]{1,0:T(8,128)} %param.7) | copy-start | bytes 393220
  1020.9 30.2 %copy-start.6 = (f32[2,128,704]{1,2,0:T(8,128)S(1)}, f32[2,128,704]{1,2,0:T(8,128)}, u32[]{:S(2)}) copy-start(f32[2,128,704]{1,2,0:T(8,128)} %param.6) | copy-start | bytes 2162692
  1046.1 5.0 copy-start.1
Sparse Core Ops, SparseCore 0:
  10.9 105.7 all-gather.12
  141.3 33.5 reduce-scatter.3
  176.6 29.8 all-gather.24
  374.0 25.5 all-gather.14
  418.7 102.1 all-gather.16
  545.4 33.5 reduce-scatter.5
  580.6 29.8 all-gather.26
  698.0 25.0 all-gather.18
  741.5 102.1 all-gather.20
  868.1 33.5 reduce-scatter.7
  903.4 29.8 all-gather.28
  1021.0 25.0 all-gather.22
